TPU v7x, 32 devices: a whole 2x2x4 slice. The times are simulated.
32 devices in a mesh: ep: 4 (over y, x), tp: 8 (over z, core).
Axes of the slice: x: 2, y: 2, z: 4, core: 2. Of those that a mesh axis runs over, the one named last changes fastest.
Arguments:
- tokens: bfloat16 [64, 2048], P('ep'), may hold values from -6 to 6
- routes: int32 [64, 4], P('ep'), may hold values from 0 to 7, all different within a row; in each aligned block of 16 rows (0 to 15, 16 to 31, ...) at most 16 rows name the same one
- route_weight: float32 [64, 4], P('ep'), may hold values from 0.2 to 1
- mixer_gain: float32 [2048], replicated, may hold values from 0.1 to 1.9
- gate_weight: bfloat16 [2048, 4096], P(None, 'tp'), may hold values from -0.125 to 0.125
- input_weight: bfloat16 [2048, 4096], P(None, 'tp'), may hold values from -0.125 to 0.125
- step_weight: bfloat16 [2048, 64], P(None, 'tp'), may hold values from -0.125 to 0.125
- write_weight: bfloat16 [2048, 512], P('tp'), may hold values from -0.125 to 0.125
- read_weight: bfloat16 [2048, 512], P('tp'), may hold values from -0.125 to 0.125
- step_bias: float32 [64], P('tp'), may hold values from -3 to 0.5
- decay_log: float32 [64], P('tp'), may hold values from -2 to 0.5
- decay_jolt: float32 [64, 64], P('ep', 'tp'), may hold values from -1 to 0
- filter_taps: bfloat16 [4, 4096], P(None, 'tp'), may hold values from -3 to 3
- filter_state: bfloat16 [64, 3, 4096], P('ep', None, 'tp'), may hold values from -6 to 6
- scan_state: float32 [64, 64, 64, 128], P('ep', 'tp'), may hold values from -2 to 2
- skip_gain: float32 [64], P('tp'), may hold values from 0.5 to 2
- head_gain: float32 [4096], P('tp'), may hold values from 0.1 to 1.9
- output_weight: bfloat16 [4096, 2048], P('tp'), may hold values from -0.09375 to 0.09375
- channel_gain: float32 [2048], replicated, may hold values from 0.1 to 1.9
- expert_gate: bfloat16 [8, 2048, 2048], P('ep', None, 'tp'), may hold values from -0.125 to 0.125
- expert_up: bfloat16 [8, 2048, 2048], P('ep', None, 'tp'), may hold values from -0.125 to 0.125
- expert_down: bfloat16 [8, 2048, 2048], P('ep', 'tp'), may hold values from -0.125 to 0.125
- shared_gate: bfloat16 [2048, 2048], P(None, 'tp'), may hold values from -0.125 to 0.125
- shared_up: bfloat16 [2048, 2048], P(None, 'tp'), may hold values from -0.125 to 0.125
- shared_down: bfloat16 [2048, 2048], P('tp'), may hold values from -0.125 to 0.125
Outputs:
- layer_out: bfloat16 [64, 2048], P('ep', 'tp')
- new_state: float32 [64, 64, 64, 128], P('ep', 'tp')
- new_filter: bfloat16 [64, 3, 4096], P('ep', None, 'tp')
Inputs may be any that keep to these rules, and one draw needn't show every extreme that they name: `routes`: each row names 4 different experts. In each aligned block of 16 rows (the rows of one index of ep) no expert is named by more than 16 rows, a bound that some block reaches.
All inputs are finite; a program needn't handle non-finite values.
Results may differ from a plain program's by a relative error of at most 0.025.
Values may be sent and summed in bfloat16 or wider, within the bound.
A program may use at most 64 MiB of HBM per device.

v0:
```python
import jax
import jax.numpy as jnp
from jax import lax
from jax.sharding import PartitionSpec as P

HEADS = 64
HEAD_DIM = 64
GROUPS = 4
STATE = 128
EPS = 1e-06


def rms_normed(values, scaling):
    mean_square = jnp.mean(values * values, axis=-1, keepdims=True)
    return values * lax.rsqrt(mean_square + EPS) * scaling


def route_targets(route_ids, experts, capacity):
    count_rows, top_picks = route_ids.shape
    flattened = route_ids.reshape(count_rows * top_picks)
    onehot = (flattened[:, None] == jnp.arange(experts, dtype=jnp.int32)[None, :]).astype(jnp.int32)
    before = jnp.cumsum(onehot, axis=0) - onehot
    slot_index = jnp.sum(before * onehot, axis=1)
    return (flattened * capacity + slot_index).reshape(count_rows, top_picks)


def expert_terms(token_rows, expert_gate, expert_up, expert_down):
    gate_part = jnp.einsum(
        "ajcd,jdf->ajcf", token_rows, expert_gate, preferred_element_type=jnp.float32
    )
    up_part = jnp.einsum(
        "ajcd,jdf->ajcf", token_rows, expert_up, preferred_element_type=jnp.float32
    )
    hidden = (jax.nn.silu(gate_part) * up_part).astype(jnp.bfloat16)
    return jnp.einsum("ajcf,jfd->ajcd", hidden, expert_down, preferred_element_type=jnp.float32)


def on_device(
    tokens,
    routes,
    route_weight,
    mixer_gain,
    gate_weight,
    input_weight,
    step_weight,
    write_weight,
    read_weight,
    step_bias,
    decay_log,
    decay_jolt,
    filter_taps,
    filter_state,
    scan_state,
    skip_gain,
    head_gain,
    output_weight,
    channel_gain,
    expert_gate,
    expert_up,
    expert_down,
    shared_gate,
    shared_up,
    shared_down,
):
    seq_rows, model_width = tokens.shape
    tp_count = lax.axis_size("tp")
    tp_index = lax.axis_index("tp")
    ep_count = lax.axis_size("ep")
    col_count = model_width // tp_count
    col_start = tp_index * col_count
    tokens_f = tokens.astype(jnp.float32)
    normed = rms_normed(tokens_f, mixer_gain).astype(jnp.bfloat16)
    feature_rows = write_weight.shape[0]
    own_features = lax.dynamic_slice_in_dim(normed, tp_index * feature_rows, feature_rows, 1)
    write_part = jnp.dot(own_features, write_weight, preferred_element_type=jnp.float32)
    read_part = jnp.dot(own_features, read_weight, preferred_element_type=jnp.float32)
    write_in, read_in = (
        lax.psum(write_part.astype(jnp.bfloat16), "tp").astype(jnp.float32),
        lax.psum(read_part.astype(jnp.bfloat16), "tp").astype(jnp.float32),
    )
    gate_rows = jnp.dot(normed, gate_weight, preferred_element_type=jnp.float32).astype(
        jnp.bfloat16
    )
    input_rows = jnp.dot(normed, input_weight, preferred_element_type=jnp.float32).astype(
        jnp.bfloat16
    )
    step_raw = jnp.dot(normed, step_weight, preferred_element_type=jnp.float32)
    window = jnp.concatenate([filter_state, input_rows[:, None, :]], axis=1)
    filtered = jax.nn.silu(
        jnp.sum(window.astype(jnp.float32) * filter_taps.astype(jnp.float32)[None], axis=1)
    )
    step_size = jax.nn.softplus(step_raw + step_bias)
    log_decay = decay_jolt - jnp.exp(decay_log) * step_size
    heads_here = step_bias.shape[0]
    head_input = filtered.reshape(seq_rows, heads_here, HEAD_DIM)
    group_index = tp_index * heads_here // (HEADS // GROUPS)
    write_vec = jax.nn.silu(lax.dynamic_slice_in_dim(write_in, group_index * STATE, STATE, 1))
    read_vec = jax.nn.silu(lax.dynamic_slice_in_dim(read_in, group_index * STATE, STATE, 1))
    new_state = (
        jnp.exp(log_decay)[:, :, None, None] * scan_state
        + (step_size[:, :, None] * head_input)[:, :, :, None] * write_vec[:, None, None, :]
    )
    readout = jnp.einsum("shpn,sn->shp", new_state, read_vec, precision=lax.Precision.HIGHEST)
    readout = readout + skip_gain[None, :, None] * head_input
    gate_heads = gate_rows.astype(jnp.float32).reshape(seq_rows, heads_here, HEAD_DIM)
    gated = rms_normed(readout * jax.nn.silu(gate_heads), head_gain.reshape(heads_here, HEAD_DIM))
    gated = gated.astype(jnp.bfloat16).reshape(seq_rows, heads_here * HEAD_DIM)
    mixer_part = jnp.dot(gated, output_weight, preferred_element_type=jnp.float32)
    mixed = lax.psum(mixer_part.astype(jnp.bfloat16), "tp")
    resid = (tokens_f + mixed.astype(jnp.float32)).astype(jnp.bfloat16)
    normed_ffn = rms_normed(resid.astype(jnp.float32), channel_gain).astype(jnp.bfloat16)
    resid_own = lax.dynamic_slice_in_dim(resid, col_start, col_count, 1)
    shared_hidden = (
        jax.nn.silu(jnp.dot(normed_ffn, shared_gate, preferred_element_type=jnp.float32))
        * jnp.dot(normed_ffn, shared_up, preferred_element_type=jnp.float32)
    ).astype(jnp.bfloat16)
    shared_part = jnp.dot(shared_hidden, shared_down, preferred_element_type=jnp.float32)
    local_experts = expert_gate.shape[0]
    experts = local_experts * ep_count
    top_picks = routes.shape[1]
    capacity = 2 * seq_rows * top_picks // experts
    targets = route_targets(routes, experts, capacity)
    slot_ids = jnp.arange(experts * capacity, dtype=jnp.int32)
    dispatch = jnp.sum((targets[None, :, :] == slot_ids[:, None, None]).astype(jnp.float32), axis=2)
    send_rows = jnp.dot(
        dispatch.astype(jnp.bfloat16), normed_ffn, preferred_element_type=jnp.float32
    )
    send_rows = send_rows.astype(jnp.bfloat16).reshape(
        ep_count, local_experts, capacity, model_width
    )
    terms = expert_terms(
        lax.all_to_all(send_rows, "ep", split_axis=0, concat_axis=0, tiled=True),
        expert_gate,
        expert_up,
        expert_down,
    )
    routed_parts, shared_sum = (
        lax.psum_scatter(terms.astype(jnp.bfloat16), "tp", scatter_dimension=3, tiled=True).astype(
            jnp.float32
        ),
        lax.psum_scatter(
            shared_part.reshape(1, 1, seq_rows, model_width).astype(jnp.bfloat16),
            "tp",
            scatter_dimension=3,
            tiled=True,
        ).astype(jnp.float32),
    )
    expert_rows = routed_parts.astype(jnp.bfloat16)
    returned = lax.all_to_all(expert_rows, "ep", split_axis=0, concat_axis=0, tiled=True)
    returned = returned.reshape(experts * capacity, col_count).astype(jnp.float32)
    combine = jnp.sum(
        jnp.where(targets[:, :, None] == slot_ids[None, None, :], route_weight[:, :, None], 0.0),
        axis=1,
    )
    routed_sum = jnp.dot(combine, returned, precision=lax.Precision.HIGHEST)
    layer_out = (resid_own.astype(jnp.float32) + shared_sum[0, 0] + routed_sum).astype(jnp.bfloat16)
    return (layer_out, new_state, window[:, 1:, :])


def solution(mesh):
    in_specs = (
        P("ep", None),
        P("ep", None),
        P("ep", None),
        P(),
        P(None, "tp"),
        P(None, "tp"),
        P(None, "tp"),
        P("tp", None),
        P("tp", None),
        P("tp"),
        P("tp"),
        P("ep", "tp"),
        P(None, "tp"),
        P("ep", None, "tp"),
        P("ep", "tp", None, None),
        P("tp"),
        P("tp"),
        P("tp", None),
        P(),
        P("ep", None, "tp"),
        P("ep", None, "tp"),
        P("ep", "tp", None),
        P(None, "tp"),
        P(None, "tp"),
        P("tp", None),
    )
    out_specs = (P("ep", "tp"), P("ep", "tp", None, None), P("ep", None, "tp"))
    return jax.shard_map(
        on_device, mesh=mesh, in_specs=in_specs, out_specs=out_specs, check_vma=False
    )
```

profile of v0, /device:TPU:0, one launch (start us, length us, event | category | flops | bytes accessed | tf_op | source)
XLA Modules:
  0.0 199.6 jit_solution(1012858224445261043)
XLA Ops:
  7.2 0.0 copy-start
  7.2 0.0 copy-start.3
  7.2 0.0 copy-start.4
  7.2 0.0 copy-start.14
  7.2 0.0 copy-start.13
  7.2 0.0 copy-start.15
  7.2 0.0 copy-start.12
  7.2 0.0 all-reduce.3.cloned.1.call-start
  7.3 1.1 fusion.31
  8.4 0.9 fusion.33
  9.4 0.0 copy-start.8
  9.4 0.0 copy-start.5
  9.4 2.0 fusion.21
  11.4 0.1 reshape.93
  11.5 0.1 convolution_convert_fusion.6
  11.6 0.2 convolution_convert_fusion.5
  11.8 0.0 copy-done.13
  11.8 0.1 subtract_exponential_fusion
  11.9 0.1 copy.59
  12.0 2.0 fusion.22
  14.1 0.1 reduce_sum.69
  14.1 0.1 copy.58
  14.2 0.1 mul.206
  14.3 30.3 %all-reduce = (bf16[16,512]{1,0:T(8,128)(2,1)S(1)}, bf16[16,512]{1,0:T(8,128)(2,1)S(1)}) all-reduce(bf16[16,512]{1,0:T(8,128)(2,1)S(1)} %convolution_convert_fusion.6, bf16[16,512]{1,0:T(8,128)(2,1)S(1)} %convolution_convert_fusion.5), channel_id=1, replica_groups=mesh['ep'=4,'tp'=8] {'tp'}, use_global_device_ids=true, to_apply=%region_2.0 | all-reduce | flops 16384 | bytes 65536 | tf_op jit(solution)/shard_map/psum | solution.py:78
  44.6 0.1 broadcast_multiply_fusion
  44.7 3.1 %multiply_add_fusion = f32[16,8,64,128]{3,2,1,0:T(8,128)S(1)} fusion(f32[16,8,64,128]{3,2,1,0:T(8,128)} %param.39, f32[16,128]{1,0:T(8,128)S(1)} %get-tuple-element.12, f32[16,8,64]{2,1,0:T(8,128)S(1)} %broadcast_multiply_fusion, f32[16,8]{1,0:T(8,128)S(1)} %copy.58), kind=kLoop, calls=%fused_computation | loop fusion | flops 3145728 | bytes 8430080 | tf_op jit(solution)/shard_map/add | solution.py:100
  47.8 0.0 copy-start.1
  47.8 0.0 copy-start.11
  47.8 9.8 %fusion.68 = f32[16,1,8,64]{3,1,2,0:T(1,128)S(1)} fusion(f32[16,8,64,128]{3,2,1,0:T(8,128)S(1)} %multiply_add_fusion, f32[16,128,1,1]{1,2,3,0:T(1,128)S(1)} %bitcast.72), kind=kOutput, calls=%fused_computation.95 | convolution fusion | flops 12582912 | bytes 4235264 | tf_op jit(solution)/shard_map/shpn,sn->shp/dot_general | solution.py:103
  57.6 0.0 copy-start.2
  57.7 0.0 copy-start.6
  57.7 0.2 multiply_reduce_fusion.1
  57.9 0.1 multiply_convert_fusion
  58.0 0.1 reshape.89
  58.1 2.6 %convolution_convert_fusion.3 = bf16[16,2048]{1,0:T(8,128)(2,1)} fusion(bf16[16,512]{1,0:T(8,128)(2,1)S(1)} %reshape.89, bf16[512,2048]{1,0:T(8,128)(2,1)} %param.42), kind=kOutput, calls=%fused_computation.5 | convolution fusion | flops 33587200 | bytes 2179072 | tf_op jit(solution)/shard_map/dot_general | solution.py:108
  60.7 0.0 all-reduce.3.cloned.1.call-update
  60.7 0.0 reduce-scatter.5.cloned.1.call-start
  60.7 0.1 copy.60
  60.8 0.1 eq.20
  60.9 0.1 fusion.42
  61.0 0.1 reduce_window_sum.11
  61.1 0.2 select_reduce_fusion.1
  61.3 0.1 reduce_sum.73
  61.4 0.1 copy.61
  61.5 0.1 convert_reduce_fusion
  61.5 52.3 %all-reduce.3.cloned.1.call-done = bf16[16,2048]{1,0:T(8,128)(2,1)} async-done(((bf16[16,2048]{1,0:T(8,128)(2,1)}), bf16[16,2048]{1,0:T(8,128)(2,1)}) %all-reduce.3.cloned.1.call-update) | async-done | bytes 65552 | tf_op jit(solution)/shard_map/psum | solution.py:109
  113.9 1.0 fusion.28
  114.9 0.3 convolution_convert_fusion.1
  115.2 10.6 %all_to_all.10 = bf16[4,2,16,2048]{3,2,1,0:T(8,128)(2,1)S(1)} all-to-all(bf16[4,2,16,2048]{3,2,1,0:T(8,128)(2,1)S(1)} %bitcast.69), channel_id=1, replica_groups=mesh['ep'=4,'tp'=8] {'ep'}, dimensions={0} | all-to-all | bytes 1048576 | tf_op jit(solution)/shard_map/all_to_all | solution.py:132
  125.8 2.1 %fusion.7 = f32[4,2,16,256]{3,2,0,1:T(8,128)S(1)} fusion(bf16[2,2048,256]{2,1,0:T(8,128)(2,1)} %param.44, bf16[4,2,16,2048]{3,2,1,0:T(8,128)(2,1)S(1)} %all_to_all.10), kind=kOutput, calls=%fused_computation.12 | convolution fusion | flops 134217728 | bytes 2752512 | tf_op jit(solution)/shard_map/ajcd,jdf->ajcf/dot_general | solution.py:28
  127.8 3.3 %fusion = bf16[4,2,16,2048]{3,2,0,1:T(8,128)(2,1)} fusion(bf16[2,256,2048]{2,1,0:T(8,128)(2,1)S(1)} %copy-done, bf16[2,2048,256]{2,1,0:T(8,128)(2,1)} %param.45, bf16[4,2,16,2048]{3,2,1,0:T(8,128)(2,1)S(1)} %all_to_all.10, f32[4,2,16,256]{3,2,0,1:T(8,128)S(1)} %fusion.7), kind=kOutput, calls=%fused_computation.3 | convolution fusion | flops 268894208 | bytes 5373952 | tf_op jit(solution)/shard_map/ajcf,jfd->ajcd/dot_general | solution.py:35
  131.1 0.0 reduce-scatter.5.cloned.1.call-update
  131.1 0.0 reduce-scatter.3.cloned.1.call-start
  131.2 1.5 fusion.65
  132.7 2.9 %fusion.1 = bf16[1,1,16,2048]{3,2,1,0:T(8,128)(2,1)} fusion(bf16[256,2048]{1,0:T(8,128)(2,1)} %param.49, bf16[2048,256]{1,0:T(8,128)(2,1)} %param.48, f32[16,256]{1,0:T(8,128)S(1)} %fusion.65, bf16[16,2048]{1,0:T(8,128)(2,1)S(1)} %get-tuple-element.6, f32[2048]{0:T(1024)S(1)} %copy-done.6, f32[16]{0:T(128)S(1)} %add_rsqrt_fusion.1), kind=kOutput, calls=%fused_computation.6 | convolution fusion | flops 33742848 | bytes 2252864 | tf_op jit(solution)/shard_map/dot_general | solution.py:117
  135.6 0.0 reduce-scatter.3.cloned.1.call-update
  135.7 0.1 select_reduce_fusion
  135.8 25.0 %reduce-scatter.5.cloned.1.call-done = bf16[4,2,16,256]{3,2,0,1:T(8,128)(2,1)} async-done(((bf16[4,2,16,2048]{3,2,0,1:T(8,128)(2,1)}), bf16[4,2,16,256]{3,2,0,1:T(8,128)(2,1)}) %reduce-scatter.5.cloned.1.call-update) | async-done | bytes 65552 | tf_op jit(solution)/shard_map/reduce_scatter | solution.py:138
  160.8 1.5 copy.64
  162.2 3.6 %all-to-all-start.1 = ((bf16[4,2,16,256]{3,2,1,0:T(8,128)(2,1)}), bf16[4,2,16,256]{3,2,1,0:T(8,128)(2,1)S(1)}, u32[]{:S(2)}, u32[]{:S(2)}) async-start(bf16[4,2,16,256]{3,2,1,0:T(8,128)(2,1)} %copy.64), calls=%async_computation.3 | async-start | bytes 131072 | tf_op jit(solution)/shard_map/all_to_all | solution.py:149
  165.9 0.6 fusion.41
  166.5 25.2 %reduce-scatter.3.cloned.1.call-done = bf16[1,1,16,256]{3,2,1,0:T(8,128)(2,1)} async-done(((bf16[1,1,16,2048]{3,2,1,0:T(8,128)(2,1)}), bf16[1,1,16,256]{3,2,1,0:T(8,128)(2,1)}) %reduce-scatter.3.cloned.1.call-update) | async-done | bytes 8208 | tf_op jit(solution)/shard_map/reduce_scatter | solution.py:141
  191.7 0.0 all-to-all-done.1
  191.7 1.4 fusion.24
  (26 shorter events, 0.1 us)
Async XLA Ops:
  7.2 120.7 %copy-start = (bf16[2,256,2048]{2,1,0:T(8,128)(2,1)S(1)}, bf16[2,256,2048]{2,1,0:T(8,128)(2,1)}, u32[]{:S(2)}) copy-start(bf16[2,256,2048]{2,1,0:T(8,128)(2,1)} %param.46) | copy-start | bytes 6291460
  7.2 4.3 %copy-start.3 = (bf16[256,512]{1,0:T(8,128)(2,1)S(1)}, bf16[256,512]{1,0:T(8,128)(2,1)}, u32[]{:S(2)}) copy-start(bf16[256,512]{1,0:T(8,128)(2,1)} %param.32) | copy-start | bytes 786436
  7.2 4.4 %copy-start.4 = (bf16[256,512]{1,0:T(8,128)(2,1)S(1)}, bf16[256,512]{1,0:T(8,128)(2,1)}, u32[]{:S(2)}) copy-start(bf16[256,512]{1,0:T(8,128)(2,1)} %param.33) | copy-start | bytes 786436
  7.2 4.6 %copy-start.14 = (f32[8]{0:T(128)S(1)}, f32[8]{0:T(128)}, u32[]{:S(2)}) copy-start(f32[8]{0:T(128)} %param.35) | copy-start | bytes 100
  7.2 4.6 %copy-start.13 = (f32[16,8]{0,1:T(8,128)S(1)}, f32[16,8]{0,1:T(8,128)}, u32[]{:S(2)}) copy-start(f32[16,8]{0,1:T(8,128)} %param.36) | copy-start | bytes 1540
  7.2 4.6 %copy-start.15 = (f32[8]{0:T(128)S(1)}, f32[8]{0:T(128)}, u32[]{:S(2)}) copy-start(f32[8]{0:T(128)} %param.34) | copy-start | bytes 100
  7.2 4.6 %copy-start.12 = (bf16[2048,8]{0,1:T(8,128)(2,1)S(1)}, bf16[2048,8]{0,1:T(8,128)(2,1)}, u32[]{:S(2)}) copy-start(bf16[2048,8]{0,1:T(8,128)(2,1)} %param.31) | copy-start | bytes 98308
  7.2 106.6 %all-reduce.3.cloned.1.call-start = ((), (), s32[]{:S(2)}) async-start(), calls=%async_computation.4 | async-start | bytes 131072 | tf_op jit(solution)/shard_map/psum | solution.py:109
  9.4 4.6 %copy-start.8 = (bf16[4,512]{1,0:T(4,128)(2,1)S(1)}, bf16[4,512]{1,0:T(4,128)(2,1)}, u32[]{:S(2)}) copy-start(bf16[4,512]{1,0:T(4,128)(2,1)} %param.37) | copy-start | bytes 12292
  9.4 4.7 %copy-start.5 = (bf16[16,3,512]{2,0,1:T(8,128)(2,1)S(1)}, bf16[16,3,512]{2,0,1:T(8,128)(2,1)}, u32[]{:S(2)}) copy-start(bf16[16,3,512]{2,0,1:T(8,128)(2,1)} %param.38) | copy-start | bytes 147460
  11.4 2.8 %copy-start.9 = (f32[512]{0:T(512)S(1)}, f32[512]{0:T(512)}, u32[]{:S(2)}) copy-start(f32[512]{0:T(512)} %param.41) | copy-start | bytes 6148
  47.8 9.8 %copy-start.1 = (f32[16,8,64,128]{3,2,1,0:T(8,128)}, f32[16,8,64,128]{3,2,1,0:T(8,128)S(1)}, u32[]{:S(2)}) copy-start(f32[16,8,64,128]{3,2,1,0:T(8,128)S(1)} %multiply_add_fusion) | copy-start | bytes 12582916
  47.8 9.9 %copy-start.11 = (f32[8]{0:T(128)S(1)}, f32[8]{0:T(128)}, u32[]{:S(2)}) copy-start(f32[8]{0:T(128)} %param.40) | copy-start | bytes 100
  57.6 3.1 %copy-start.7 = (s32[16,4]{0,1:T(4,128)S(1)}, s32[16,4]{0,1:T(4,128)}, u32[]{:S(2)}) copy-start(s32[16,4]{0,1:T(4,128)} %param.26) | copy-start | bytes 772
  57.6 56.2 %copy-start.2 = (bf16[16,2048]{1,0:T(8,128)(2,1)S(1)}, bf16[16,2048]{1,0:T(8,128)(2,1)}, u32[]{:S(2)}) copy-start(bf16[16,2048]{1,0:T(8,128)(2,1)} %param.25) | copy-start | bytes 196612
  57.7 57.2 %copy-start.6 = (f32[2048]{0:T(1024)S(1)}, f32[2048]{0:T(1024)}, u32[]{:S(2)}) copy-start(f32[2048]{0:T(1024)} %param.43) | copy-start | bytes 24580
  60.7 100.1 %reduce-scatter.5.cloned.1.call-start = ((), (), s32[]{:S(2)}) async-start(), calls=%async_computation.6 | async-start | bytes 589824 | tf_op jit(solution)/shard_map/reduce_scatter | solution.py:138
  131.1 4.6 %copy-start.10 = (f32[16,4]{0,1:T(4,128)S(1)}, f32[16,4]{0,1:T(4,128)}, u32[]{:S(2)}) copy-start(f32[16,4]{0,1:T(4,128)} %param.27) | copy-start | bytes 772
  131.1 60.5 %reduce-scatter.3.cloned.1.call-start = ((), (), s32[]{:S(2)}) async-start(), calls=%async_computation.5 | async-start | bytes 73728 | tf_op jit(solution)/shard_map/reduce_scatter | solution.py:141
  162.2 29.4 %all-to-all-start.1 = ((bf16[4,2,16,256]{3,2,1,0:T(8,128)(2,1)}), bf16[4,2,16,256]{3,2,1,0:T(8,128)(2,1)S(1)}, u32[]{:S(2)}, u32[]{:S(2)}) async-start(bf16[4,2,16,256]{3,2,1,0:T(8,128)(2,1)} %copy.64), calls=%async_computation.3 | async-start | bytes 131072 | tf_op jit(solution)/shard_map/all_to_all | solution.py:149
Sparse Core Ops, SparseCore 0:
  60.8 53.0 all-reduce.2
  131.3 29.4 reduce-scatter.4
  163.0 28.6 reduce-scatter.2
where the time goes:
time: 200 us
  waiting for transfers between devices  103 us (52%)
  blocking collectives  40.9 us (20%)
  matrix products  28.4 us (14%)
  between operations  14 us (7%)
  other arithmetic  7.67 us (4%)
  starting transfers between devices  3.77 us (2%)
  local copies, waits for them, and re-layouts  2.39 us (1%)
    psum x1, waiting for transfers between devices, on_device(): mixed = lax.psum(mixer_part.astype(jnp.bfloat16), 'tp')  52.3 us
    psum x1, blocking collectives, on_device(): lax.psum(write_part.astype(jnp.bfloat16), 'tp').astype(jnp.float32)  30.3 us
    reduce_scatter x1, waiting for transfers between devices, on_device(): lax.psum_scatter(shared_part.reshape(1, 1, seq_rows, model_width).astype(...  25.2 us
    reduce_scatter x1, waiting for transfers between devices, on_device(): lax.psum_scatter(terms.astype(jnp.bfloat16), 'tp', scatter_dimension=3, t...  25 us
    all_to_all x1, blocking collectives, on_device(): lax.all_to_all(send_rows, 'ep', split_axis=0, concat_axis=0, tiled=True)  10.6 us
    dot_general x1, matrix products, on_device(): jnp.einsum('shpn,sn->shp', new_state, read_vec, precision=lax.Precision.H...  9.81 us
  transfers between devices with their start and end apart: 4, of which 3 were waited for; matrix products, arithmetic and copies ran while one was open for 4% of the time, Pallas kernels for 0%

commit v1 on v0

--- a/solution.py
+++ b/solution.py
@@ -106,7 +106,8 @@
     gated = rms_normed(readout * jax.nn.silu(gate_heads), head_gain.reshape(heads_here, HEAD_DIM))
     gated = gated.astype(jnp.bfloat16).reshape(seq_rows, heads_here * HEAD_DIM)
     mixer_part = jnp.dot(gated, output_weight, preferred_element_type=jnp.float32)
-    mixed = lax.psum(mixer_part.astype(jnp.bfloat16), "tp")
+    body = mixer_part.astype(jnp.bfloat16)
+    mixed = jnp.sum(lax.all_gather(body, "tp"), axis=0)
     resid = (tokens_f + mixed.astype(jnp.float32)).astype(jnp.bfloat16)
     normed_ffn = rms_normed(resid.astype(jnp.float32), channel_gain).astype(jnp.bfloat16)
     resid_own = lax.dynamic_slice_in_dim(resid, col_start, col_count, 1)

time: 200 us -> 164 us (0.82)
  waiting for transfers between devices: 103 us -> 49 us
  blocking collectives: 40.9 us -> 57.8 us
    psum x1 -> x0, waiting for transfers between devices: 52.3 us -> none  [on_device(): mixed = lax.psum(mixer_part.astype(jnp.bfloat16), 'tp')]
    all_gather x0 -> x1, blocking collectives: none -> 14.9 us  [on_device(): mixed = jnp.sum(lax.all_gather(body, 'tp'), axis=0)]
  transfers between devices with their start and end apart: 4 -> 3, of which waited for: 3 -> 2; matrix products, arithmetic and copies ran while one was open for 4% -> 4% of each run, Pallas kernels for 0% -> 0%
where the time goes in v1:
time: 164 us; the launch traced here: 163 us
  blocking collectives  57.8 us (35%)
  waiting for transfers between devices  49 us (30%)
  matrix products  27.8 us (17%)
  between operations  14.3 us (9%)
  other arithmetic  7.45 us (5%)
  starting transfers between devices  3.58 us (2%)
  local copies, waits for them, and re-layouts  3.21 us (2%)
    psum x1, blocking collectives, on_device(): lax.psum(write_part.astype(jnp.bfloat16), 'tp').astype(jnp.float32)  30.3 us
    reduce_scatter x1, waiting for transfers between devices, on_device(): lax.psum_scatter(shared_part.reshape(1, 1, seq_rows, model_width).astype(...  25.3 us
    reduce_scatter x1, waiting for transfers between devices, on_device(): lax.psum_scatter(terms.astype(jnp.bfloat16), 'tp', scatter_dimension=3, t...  23.7 us
    all_gather x1, blocking collectives, on_device(): mixed = jnp.sum(lax.all_gather(body, 'tp'), axis=0)  14.9 us
    all_to_all x1, blocking collectives, on_device(): lax.all_to_all(send_rows, 'ep', split_axis=0, concat_axis=0, tiled=True)  12.5 us
    dot_general x1, matrix products, on_device(): jnp.einsum('shpn,sn->shp', new_state, read_vec, precision=lax.Precision.H...  9.81 us
    all_to_all x1, starting transfers between devices, on_device(): lax.all_to_all(expert_rows, 'ep', split_axis=0, concat_axis=0, tiled=True)  3.5 us
    dot_general x1, matrix products, expert_terms(): jnp.einsum('ajcf,jfd->ajcd', hidden, expert_down, preferred_element_type=...  3.28 us
  transfers between devices with their start and end apart: 3, of which 2 were waited for; matrix products, arithmetic and copies ran while one was open for 4% of the time, Pallas kernels for 0%

profile of v1, /device:TPU:0, one launch (start us, length us, event | category | flops | bytes accessed | tf_op | source)
XLA Modules:
  0.0 163.2 jit_solution(2125472602924894963)
XLA Ops:
  7.2 0.0 copy-start
  7.2 0.0 copy-start.3
  7.2 0.0 copy-start.4
  7.2 0.0 copy-start.13
  7.2 0.0 copy-start.12
  7.2 0.0 copy-start.14
  7.2 0.0 copy-start.11
  7.2 0.0 reduce-scatter.5.cloned.1.call-start
  7.3 0.9 copy.60
  8.2 0.1 eq.20
  8.3 0.1 fusion.42
  8.4 0.1 reduce_window_sum.11
  8.5 0.2 select_reduce_fusion.1
  8.7 0.1 reduce_sum.86
  8.7 0.1 copy.61
  8.8 0.7 multiply_add_fusion.1
  9.5 0.1 convert_reduce_fusion
  9.6 1.0 fusion.31
  10.6 0.9 fusion.33
  11.5 0.0 copy-start.7
  11.5 0.0 copy-start.5
  11.5 2.0 %fusion.21 = f32[16,512]{1,0:T(8,128)S(1)} fusion(bf16[16,2048]{1,0:T(8,128)(2,1)S(1)} %fusion.33, bf16[2048,512]{1,0:T(8,128)(2,1)} %param.29), kind=kOutput, calls=%fused_computation.17 | convolution fusion | flops 33570816 | bytes 2195456 | tf_op jit(solution)/shard_map/dot_general | solution.py:81
  13.5 0.1 reshape.93
  13.6 0.0 copy-done.3
  13.6 0.1 convolution_convert_fusion.6
  13.8 0.2 convolution_convert_fusion.5
  13.9 0.0 copy-done.12
  14.0 0.1 subtract_exponential_fusion
  14.1 0.1 copy.59
  14.2 2.0 %fusion.22 = bf16[16,1,512]{2,0,1:T(8,128)(2,1)S(1)} fusion(bf16[16,2048]{1,0:T(8,128)(2,1)S(1)} %fusion.33, bf16[2048,512]{1,0:T(8,128)(2,1)} %param.30), kind=kOutput, calls=%fused_computation.21 | convolution fusion | flops 33562624 | bytes 2179072 | tf_op jit(solution)/shard_map/dot_general | solution.py:84
  16.2 0.1 reduce_sum.81
  16.3 0.1 copy.58
  16.4 0.1 mul.206
  16.4 30.3 %all-reduce = (bf16[16,512]{1,0:T(8,128)(2,1)S(1)}, bf16[16,512]{1,0:T(8,128)(2,1)S(1)}) all-reduce(bf16[16,512]{1,0:T(8,128)(2,1)S(1)} %convolution_convert_fusion.6, bf16[16,512]{1,0:T(8,128)(2,1)S(1)} %convolution_convert_fusion.5), channel_id=1, replica_groups=mesh['ep'=4,'tp'=8] {'tp'}, use_global_device_ids=true, to_apply=%region_2.0 | all-reduce | flops 16384 | bytes 65536 | tf_op jit(solution)/shard_map/psum | solution.py:78
  46.7 0.1 broadcast_multiply_fusion
  46.9 3.1 %multiply_add_fusion = f32[16,8,64,128]{3,2,1,0:T(8,128)S(1)} fusion(f32[16,8,64,128]{3,2,1,0:T(8,128)} %param.39, f32[16,128]{1,0:T(8,128)S(1)} %get-tuple-element.12, f32[16,8,64]{2,1,0:T(8,128)S(1)} %broadcast_multiply_fusion, f32[16,8]{1,0:T(8,128)S(1)} %copy.58), kind=kLoop, calls=%fused_computation | loop fusion | flops 3145728 | bytes 8430080 | tf_op jit(solution)/shard_map/add | solution.py:100
  49.9 0.0 copy-start.1
  50.0 0.0 copy-start.10
  50.0 9.8 %fusion.68 = f32[16,1,8,64]{3,1,2,0:T(1,128)S(1)} fusion(f32[16,8,64,128]{3,2,1,0:T(8,128)S(1)} %multiply_add_fusion, f32[16,128,1,1]{1,2,3,0:T(1,128)S(1)} %bitcast.74), kind=kOutput, calls=%fused_computation.95 | convolution fusion | flops 12582912 | bytes 4235264 | tf_op jit(solution)/shard_map/shpn,sn->shp/dot_general | solution.py:103
  59.8 0.0 copy-start.6
  59.8 0.2 multiply_reduce_fusion.1
  60.0 0.1 multiply_convert_fusion
  60.1 0.1 reshape.89
  60.2 2.0 %convolution_convert_fusion.3 = bf16[16,2048]{1,0:T(8,128)(2,1)S(1)} fusion(bf16[16,512]{1,0:T(8,128)(2,1)S(1)} %reshape.89, bf16[512,2048]{1,0:T(8,128)(2,1)} %param.42), kind=kOutput, calls=%fused_computation.5 | convolution fusion | flops 33587200 | bytes 2179072 | tf_op jit(solution)/shard_map/dot_general | solution.py:108
  62.2 14.9 %all-gather = bf16[128,2048]{1,0:T(8,128)(2,1)S(1)} all-gather(bf16[16,2048]{1,0:T(8,128)(2,1)S(1)} %convolution_convert_fusion.3), channel_id=2, replica_groups=mesh['ep'=4,'tp'=8] {'tp'}, dimensions={0}, use_global_device_ids=true | all-gather | bytes 589824 | tf_op jit(solution)/shard_map/all_gather | solution.py:110
  77.1 0.1 reduce_sum.83
  77.2 0.1 fusion.28
  77.4 0.3 convolution_convert_fusion.1
  77.7 12.5 %all_to_all.10 = bf16[4,2,16,2048]{3,2,1,0:T(8,128)(2,1)S(1)} all-to-all(bf16[4,2,16,2048]{3,2,1,0:T(8,128)(2,1)S(1)} %bitcast.71), channel_id=1, replica_groups=mesh['ep'=4,'tp'=8] {'ep'}, dimensions={0} | all-to-all | bytes 1048576 | tf_op jit(solution)/shard_map/all_to_all | solution.py:133
  90.2 2.1 %fusion.7 = f32[4,2,16,256]{3,2,0,1:T(8,128)S(1)} fusion(bf16[2,2048,256]{2,1,0:T(8,128)(2,1)} %param.44, bf16[4,2,16,2048]{3,2,1,0:T(8,128)(2,1)S(1)} %all_to_all.10), kind=kOutput, calls=%fused_computation.12 | convolution fusion | flops 134217728 | bytes 2752512 | tf_op jit(solution)/shard_map/ajcd,jdf->ajcf/dot_general | solution.py:28
  92.3 3.3 %fusion = bf16[4,2,16,2048]{3,2,0,1:T(8,128)(2,1)} fusion(bf16[2,256,2048]{2,1,0:T(8,128)(2,1)S(1)} %copy-done, bf16[2,2048,256]{2,1,0:T(8,128)(2,1)} %param.45, bf16[4,2,16,2048]{3,2,1,0:T(8,128)(2,1)S(1)} %all_to_all.10, f32[4,2,16,256]{3,2,0,1:T(8,128)S(1)} %fusion.7), kind=kOutput, calls=%fused_computation.3 | convolution fusion | flops 268894208 | bytes 5373952 | tf_op jit(solution)/shard_map/ajcf,jfd->ajcd/dot_general | solution.py:35
  95.6 0.0 reduce-scatter.5.cloned.1.call-update
  95.6 0.0 reduce-scatter.3.cloned.1.call-start
  95.7 1.5 fusion.65
  97.2 3.0 %fusion.1 = bf16[1,1,16,2048]{3,2,1,0:T(8,128)(2,1)} fusion(bf16[256,2048]{1,0:T(8,128)(2,1)} %param.49, bf16[2048,256]{1,0:T(8,128)(2,1)} %param.48, f32[16,256]{1,0:T(8,128)S(1)} %fusion.65, bf16[16,2048]{1,0:T(8,128)(2,1)S(1)} %get-tuple-element.6, f32[2048]{0:T(1024)S(1)} %copy-done.6, f32[16]{0:T(128)S(1)} %add_rsqrt_fusion.1), kind=kOutput, calls=%fused_computation.6 | convolution fusion | flops 33742848 | bytes 2252864 | tf_op jit(solution)/shard_map/dot_general | solution.py:118
  100.2 0.0 reduce-scatter.3.cloned.1.call-update
  100.2 0.1 select_reduce_fusion
  100.3 23.7 %reduce-scatter.5.cloned.1.call-done = bf16[4,2,16,256]{3,2,0,1:T(8,128)(2,1)} async-done(((bf16[4,2,16,2048]{3,2,0,1:T(8,128)(2,1)}), bf16[4,2,16,256]{3,2,0,1:T(8,128)(2,1)}) %reduce-scatter.5.cloned.1.call-update) | async-done | bytes 65552 | tf_op jit(solution)/shard_map/reduce_scatter | solution.py:139
  124.0 1.5 copy.64
  125.5 3.5 %all-to-all-start.1 = ((bf16[4,2,16,256]{3,2,1,0:T(8,128)(2,1)}), bf16[4,2,16,256]{3,2,1,0:T(8,128)(2,1)S(1)}, u32[]{:S(2)}, u32[]{:S(2)}) async-start(bf16[4,2,16,256]{3,2,1,0:T(8,128)(2,1)} %copy.64), calls=%async_computation.3 | async-start | bytes 131072 | tf_op jit(solution)/shard_map/all_to_all | solution.py:150
  129.0 0.6 fusion.41
  129.6 25.3 %reduce-scatter.3.cloned.1.call-done = bf16[1,1,16,256]{3,2,1,0:T(8,128)(2,1)} async-done(((bf16[1,1,16,2048]{3,2,1,0:T(8,128)(2,1)}), bf16[1,1,16,256]{3,2,1,0:T(8,128)(2,1)}) %reduce-scatter.3.cloned.1.call-update) | async-done | bytes 8208 | tf_op jit(solution)/shard_map/reduce_scatter | solution.py:142
  154.9 0.0 all-to-all-done.1
  154.9 1.4 fusion.24
  (23 shorter events, 0.1 us)
Async XLA Ops:
  7.2 85.1 %copy-start = (bf16[2,256,2048]{2,1,0:T(8,128)(2,1)S(1)}, bf16[2,256,2048]{2,1,0:T(8,128)(2,1)}, u32[]{:S(2)}) copy-start(bf16[2,256,2048]{2,1,0:T(8,128)(2,1)} %param.46) | copy-start | bytes 6291460
  7.2 6.4 %copy-start.3 = (bf16[256,512]{1,0:T(8,128)(2,1)S(1)}, bf16[256,512]{1,0:T(8,128)(2,1)}, u32[]{:S(2)}) copy-start(bf16[256,512]{1,0:T(8,128)(2,1)} %param.32) | copy-start | bytes 786436
  7.2 6.6 %copy-start.4 = (bf16[256,512]{1,0:T(8,128)(2,1)S(1)}, bf16[256,512]{1,0:T(8,128)(2,1)}, u32[]{:S(2)}) copy-start(bf16[256,512]{1,0:T(8,128)(2,1)} %param.33) | copy-start | bytes 786436
  7.2 6.7 %copy-start.13 = (f32[8]{0:T(128)S(1)}, f32[8]{0:T(128)}, u32[]{:S(2)}) copy-start(f32[8]{0:T(128)} %param.35) | copy-start | bytes 100
  7.2 6.7 %copy-start.12 = (f32[16,8]{0,1:T(8,128)S(1)}, f32[16,8]{0,1:T(8,128)}, u32[]{:S(2)}) copy-start(f32[16,8]{0,1:T(8,128)} %param.36) | copy-start | bytes 1540
  7.2 6.7 %copy-start.14 = (f32[8]{0:T(128)S(1)}, f32[8]{0:T(128)}, u32[]{:S(2)}) copy-start(f32[8]{0:T(128)} %param.34) | copy-start | bytes 100
  7.2 6.7 %copy-start.11 = (bf16[2048,8]{0,1:T(8,128)(2,1)S(1)}, bf16[2048,8]{0,1:T(8,128)(2,1)}, u32[]{:S(2)}) copy-start(bf16[2048,8]{0,1:T(8,128)(2,1)} %param.31) | copy-start | bytes 98308
  7.2 116.8 %reduce-scatter.5.cloned.1.call-start = ((), (), s32[]{:S(2)}) async-start(), calls=%async_computation.5 | async-start | bytes 589824 | tf_op jit(solution)/shard_map/reduce_scatter | solution.py:139
  11.5 4.6 %copy-start.7 = (bf16[4,512]{1,0:T(4,128)(2,1)S(1)}, bf16[4,512]{1,0:T(4,128)(2,1)}, u32[]{:S(2)}) copy-start(bf16[4,512]{1,0:T(4,128)(2,1)} %param.37) | copy-start | bytes 12292
  11.5 4.7 %copy-start.5 = (bf16[16,3,512]{2,0,1:T(8,128)(2,1)S(1)}, bf16[16,3,512]{2,0,1:T(8,128)(2,1)}, u32[]{:S(2)}) copy-start(bf16[16,3,512]{2,0,1:T(8,128)(2,1)} %param.38) | copy-start | bytes 147460
  13.5 2.8 %copy-start.8 = (f32[512]{0:T(512)S(1)}, f32[512]{0:T(512)}, u32[]{:S(2)}) copy-start(f32[512]{0:T(512)} %param.41) | copy-start | bytes 6148
  49.9 9.8 %copy-start.1 = (f32[16,8,64,128]{3,2,1,0:T(8,128)}, f32[16,8,64,128]{3,2,1,0:T(8,128)S(1)}, u32[]{:S(2)}) copy-start(f32[16,8,64,128]{3,2,1,0:T(8,128)S(1)} %multiply_add_fusion) | copy-start | bytes 12582916
  50.0 9.9 %copy-start.10 = (f32[8]{0:T(128)S(1)}, f32[8]{0:T(128)}, u32[]{:S(2)}) copy-start(f32[8]{0:T(128)} %param.40) | copy-start | bytes 100
  59.8 17.4 %copy-start.2 = (bf16[16,2048]{1,0:T(8,128)(2,1)S(1)}, bf16[16,2048]{1,0:T(8,128)(2,1)}, u32[]{:S(2)}) copy-start(bf16[16,2048]{1,0:T(8,128)(2,1)} %param.25) | copy-start | bytes 196612
  59.8 17.6 %copy-start.6 = (f32[2048]{0:T(1024)S(1)}, f32[2048]{0:T(1024)}, u32[]{:S(2)}) copy-start(f32[2048]{0:T(1024)} %param.43) | copy-start | bytes 24580
  95.6 4.6 %copy-start.9 = (f32[16,4]{0,1:T(4,128)S(1)}, f32[16,4]{0,1:T(4,128)}, u32[]{:S(2)}) copy-start(f32[16,4]{0,1:T(4,128)} %param.27) | copy-start | bytes 772
  95.6 59.3 %reduce-scatter.3.cloned.1.call-start = ((), (), s32[]{:S(2)}) async-start(), calls=%async_computation.4 | async-start | bytes 73728 | tf_op jit(solution)/shard_map/reduce_scatter | solution.py:142
  125.5 29.4 %all-to-all-start.1 = ((bf16[4,2,16,256]{3,2,1,0:T(8,128)(2,1)}), bf16[4,2,16,256]{3,2,1,0:T(8,128)(2,1)S(1)}, u32[]{:S(2)}, u32[]{:S(2)}) async-start(bf16[4,2,16,256]{3,2,1,0:T(8,128)(2,1)} %copy.64), calls=%async_computation.3 | async-start | bytes 131072 | tf_op jit(solution)/shard_map/all_to_all | solution.py:150
Sparse Core Ops, SparseCore 0:
  95.7 28.2 reduce-scatter.4
  126.2 28.6 reduce-scatter.2
